TPU v7x, 128 devices: a whole 4x4x4 slice. The times are simulated.
128 devices in a mesh: ep: 128 (over z, y, x, core).
Axes of the slice: x: 4, y: 4, z: 4, core: 2. Of those that a mesh axis runs over, the one named last changes fastest.
Arguments:
- tokens: bfloat16 [128, 2048], P('ep'), may hold values from -6 to 6
- mixer_gain: float32 [2048], replicated, may hold values from 0.1 to 1.9
- query_weight: bfloat16 [2048, 2048], P(None, 'ep'), may hold values from -0.125 to 0.125
- key_weight: bfloat16 [2048, 2048], P(None, 'ep'), may hold values from -0.125 to 0.125
- value_weight: bfloat16 [2048, 2048], P(None, 'ep'), may hold values from -0.125 to 0.125
- outgate_weight: bfloat16 [2048, 2048], P(None, 'ep'), may hold values from -0.125 to 0.125
- input_weight: bfloat16 [2048, 4], replicated, may hold values from -0.125 to 0.125
- forget_weight: bfloat16 [2048, 4], replicated, may hold values from -0.125 to 0.125
- forget_bias: float32 [4], replicated, may hold values from 0 to 4
- memory_matrix: float32 [128, 4, 512, 512], P('ep'), may hold values from -0.3 to 0.3
- memory_norm: float32 [128, 4, 512], P('ep'), may hold values from -0.3 to 0.3
- memory_max: float32 [128, 4], P('ep'), may hold values from -2 to 2
- mixer_out: bfloat16 [2048, 2048], P(None, 'ep'), may hold values from -0.125 to 0.125
- expert_gain: float32 [2048], replicated, may hold values from 0.1 to 1.9
- expert_gate: bfloat16 [128, 2048, 1024], P('ep'), may hold values from -0.125 to 0.125
- expert_up: bfloat16 [128, 2048, 1024], P('ep'), may hold values from -0.125 to 0.125
- expert_down: bfloat16 [128, 1024, 2048], P('ep'), may hold values from -0.1875 to 0.1875
- route_group: int32 [128], P('ep'), may hold values from 0 to 3
- route_member: int32 [128, 2], P('ep'), may hold values from 0 to 31, as said below
- group_weight: float32 [128], P('ep'), may hold values from 0.25 to 1
- member_weight: float32 [128, 2], P('ep'), may hold values from 0.1 to 1
Outputs:
- layer_out: bfloat16 [128, 2048], P('ep')
- next_matrix: float32 [128, 4, 512, 512], P('ep')
- next_norm: float32 [128, 4, 512], P('ep')
- next_max: float32 [128, 4], P('ep')
Inputs may be any that keep to these rules, and one draw needn't show every extreme that they name: A row's 2 experts, numbered route_group * 32 + route_member, are different members of the one group that route_group names. No expert is named by more than 4 rows in all, and one expert is named by exactly 4 rows.
All inputs are finite; a program needn't handle non-finite values.
Results may differ from a plain program's by a relative error of at most 0.013.
Values may be sent and summed in bfloat16 or wider, within the bound.
A program may use at most 64 MiB of HBM per device.

v0:
```python
import math

import jax
import jax.numpy as jnp
from jax import lax
from jax.sharding import PartitionSpec as P

GROUPS = 4
CAPACITY = 4


norm_eps = 1e-06


def sent_together(arrays, axis, split_dim, concat_dim, along):
    widths = [math.prod(a.shape[along:]) for a in arrays]
    both = jnp.concatenate(
        [a.reshape(*a.shape[:along], w) for a, w in zip(arrays, widths)], axis=along
    )
    filled = lax.all_to_all(both, axis, split_axis=split_dim, concat_axis=concat_dim, tiled=True)
    parts = jnp.split(filled, [sum(widths[:k]) for k in range(1, len(widths))], axis=along)
    return tuple(
        (b.reshape(*filled.shape[:along], *a.shape[along:]) for a, b in zip(arrays, parts))
    )


def root_norm(values, gain):
    return values * lax.rsqrt(jnp.mean(values * values, axis=-1, keepdims=True) + norm_eps) * gain


def run_expert(slot_rows, gate_mat, up_mat, down_mat):
    gate_part = jnp.dot(slot_rows, gate_mat, preferred_element_type=jnp.float32)
    up_part = jnp.dot(slot_rows, up_mat, preferred_element_type=jnp.float32)
    hidden = (jax.nn.silu(gate_part) * up_part).astype(jnp.bfloat16)
    return jnp.dot(hidden, down_mat, preferred_element_type=jnp.float32).astype(jnp.bfloat16)


def local(
    tokens,
    mixer_gain,
    query_weight,
    key_weight,
    value_weight,
    outgate_weight,
    input_weight,
    forget_weight,
    forget_bias,
    memory_matrix,
    memory_norm,
    memory_max,
    mixer_out,
    expert_gain,
    expert_gate,
    expert_up,
    expert_down,
    route_group,
    route_member,
    group_weight,
    member_weight,
):
    devices = lax.axis_size("ep")
    local_rows = tokens.shape[0]
    width = tokens.shape[1]
    columns = query_weight.shape[1]
    heads = memory_matrix.shape[1]
    head_dim = memory_matrix.shape[2]
    members = devices * expert_gate.shape[0] // GROUPS
    stacked = jnp.concatenate([query_weight, key_weight, value_weight, outgate_weight], axis=1)
    piece = lax.all_gather(tokens, "ep", axis=0, tiled=True)
    normed = root_norm(piece.astype(jnp.float32), mixer_gain).astype(jnp.bfloat16)
    result = jnp.dot(normed, stacked, preferred_element_type=jnp.float32).astype(jnp.bfloat16)
    result = result.reshape(piece.shape[0], 4, columns)
    parts = lax.all_to_all(result, "ep", split_axis=0, concat_axis=2, tiled=True)
    resid = tokens.astype(jnp.float32)
    own_normed = root_norm(resid, mixer_gain).astype(jnp.bfloat16)
    input_pre = jnp.dot(own_normed, input_weight, preferred_element_type=jnp.float32)
    forget_pre = (
        jnp.dot(own_normed, forget_weight, preferred_element_type=jnp.float32) + forget_bias
    )
    log_forget = jax.nn.log_sigmoid(forget_pre)
    next_max = jnp.maximum(log_forget + memory_max, input_pre)
    keep = jnp.exp(log_forget + memory_max - next_max)
    admit = jnp.exp(input_pre - next_max)
    query_heads = parts[:, 0].astype(jnp.float32).reshape(local_rows, heads, head_dim)
    key_heads = parts[:, 1].astype(jnp.float32).reshape(local_rows, heads, head_dim) * head_dim ** (
        -0.5
    )
    value_heads = parts[:, 2].astype(jnp.float32).reshape(local_rows, heads, head_dim)
    carried = jnp.einsum("shij,shj->shi", memory_matrix, query_heads)
    score = jnp.sum(key_heads * query_heads, axis=-1)
    numer = keep[..., None] * carried + (admit * score)[..., None] * value_heads
    denom = keep * jnp.sum(memory_norm * query_heads, axis=-1) + admit * score
    head_out = numer / jnp.maximum(jnp.abs(denom), jnp.exp(-next_max))[..., None]
    gated = (
        head_out.reshape(local_rows, width) * jax.nn.sigmoid(parts[:, 3].astype(jnp.float32))
    ).astype(jnp.bfloat16)
    next_matrix = (
        keep[..., None, None] * memory_matrix
        + admit[..., None, None] * value_heads[..., :, None] * key_heads[..., None, :]
    )
    next_norm = keep[..., None] * memory_norm + admit[..., None] * key_heads
    proj_cols = jnp.dot(
        lax.all_gather(gated, "ep", axis=0, tiled=True),
        mixer_out,
        preferred_element_type=jnp.float32,
    ).astype(jnp.bfloat16)
    slot_index = jnp.arange(CAPACITY, dtype=jnp.int32)
    chosen_local = route_group[:, None] * members + route_member
    row_numbers = jnp.arange(local_rows, dtype=jnp.int32)
    local_weight = group_weight[:, None] * member_weight
    projected = lax.all_to_all(proj_cols, "ep", split_axis=0, concat_axis=1, tiled=True)
    middle = (resid + projected.astype(jnp.float32)).astype(jnp.bfloat16)
    expert_in = root_norm(middle.astype(jnp.float32), expert_gain).astype(jnp.bfloat16)
    targets = jnp.arange(devices, dtype=jnp.int32)
    hit = jnp.any(chosen_local[:, :, None] == targets[None, None, :], axis=1)
    outgoing = jnp.where(hit.T[:, :, None], expert_in[None, :, :], jnp.zeros((), jnp.bfloat16))
    present = hit.T.astype(jnp.bfloat16)
    incoming, flags = sent_together((outgoing, present), "ep", 0, 0, 2)
    flat_rows = incoming.reshape(devices * local_rows, width)
    live = (flags.reshape(devices * local_rows) > 0.5).astype(jnp.int32)
    position = jnp.cumsum(live) - 1
    select = ((position[None, :] == slot_index[:, None]) & (live[None, :] > 0)).astype(jnp.bfloat16)
    slot_rows = jnp.dot(select, flat_rows, preferred_element_type=jnp.float32).astype(jnp.bfloat16)
    finished = run_expert(slot_rows, expert_gate[0], expert_up[0], expert_down[0])
    back_rows = jnp.dot(select.T, finished, preferred_element_type=jnp.float32).astype(jnp.bfloat16)
    returned = lax.all_to_all(
        back_rows.reshape(devices, local_rows, width), "ep", split_axis=0, concat_axis=0, tiled=True
    )
    picked = returned[chosen_local.T, row_numbers[None, :]]
    mixture = jnp.sum(local_weight.T[:, :, None] * picked.astype(jnp.float32), axis=0)
    layer_out = (middle.astype(jnp.float32) + mixture).astype(jnp.bfloat16)
    return (layer_out, next_matrix, next_norm, next_max)


def solution(mesh):
    placed = (
        P("ep", None),
        P(),
        P(None, "ep"),
        P(None, "ep"),
        P(None, "ep"),
        P(None, "ep"),
        P(),
        P(),
        P(),
        P("ep", None, None, None),
        P("ep", None, None),
        P("ep", None),
        P(None, "ep"),
        P(),
        P("ep", None, None),
        P("ep", None, None),
        P("ep", None, None),
        P("ep"),
        P("ep", None),
        P("ep"),
        P("ep", None),
    )
    return jax.shard_map(
        local,
        mesh=mesh,
        in_specs=placed,
        out_specs=(P("ep", None), P("ep", None, None, None), P("ep", None, None), P("ep", None)),
        check_vma=False,
    )
```

profile of v0, /device:TPU:0, one launch (start us, length us, event | category | flops | bytes accessed | tf_op | source)
XLA Modules:
  0.0 176.7 jit_solution(14111888973665260234)
XLA Ops:
  0.8 38.6 %all-gather = bf16[128,1,2048]{2,1,0:T(2,128)(2,1)S(1)} all-gather(bf16[1,1,2048]{2,1,0:T(2,128)(2,1)} %bitcast.145), channel_id=1, replica_groups=mesh['ep'=128] {'ep'}, dimensions={0}, use_global_device_ids=true | all-gather | bytes 528384 | tf_op jit(solution)/shard_map/all_gather | solution.py:69
  39.4 1.1 convert_element_type.241
  40.9 0.5 convolution_convert_fusion.2
  41.4 0.8 copy.57
  42.2 6.7 %all-to-all-start = ((bf16[128,4,16]{2,1,0:T(4,128)(2,1)}), bf16[128,4,16]{2,1,0:T(4,128)(2,1)S(1)}, u32[]{:S(2)}, u32[]{:S(2)}) async-start(bf16[128,4,16]{2,1,0:T(4,128)(2,1)} %copy.57), calls=%async_computation | async-start | bytes 262144 | tf_op jit(solution)/shard_map/all_to_all | solution.py:73
  48.9 0.6 multiply_reduce_fusion.4
  51.3 7.0 %all-to-all-done = bf16[128,4,16]{2,1,0:T(4,128)(2,1)S(1)} async-done(((bf16[128,4,16]{2,1,0:T(4,128)(2,1)}), bf16[128,4,16]{2,1,0:T(4,128)(2,1)S(1)}, u32[]{:S(2)}, u32[]{:S(2)}) %all-to-all-start) | async-done | bytes 16416 | tf_op jit(solution)/shard_map/all_to_all | solution.py:73
  58.6 2.8 %fusion.72 = f32[4,1,512]{2,1,0:T(1,128)S(1)} fusion(bf16[4,512,1]{1,2,0:T(2,128)(2,1)S(1)} %bitcast.147, f32[1,4,512,512]{3,2,1,0:T(8,128)} %param.30), kind=kOutput, calls=%fused_computation.111 | convolution fusion | flops 2097152 | bytes 4206592 | tf_op jit(solution)/shard_map/shij,shj->shi/dot_general | solution.py:89
  61.5 0.8 multiply_reduce_fusion.3
  62.5 34.2 %all-gather.1 = bf16[128,1,2048]{2,1,0:T(2,128)(2,1)S(1)} all-gather(bf16[1,1,2048]{2,1,0:T(2,128)(2,1)S(1)} %convert_bitcast_fusion), channel_id=1, replica_groups=mesh['ep'=128] {'ep'}, dimensions={0}, use_global_device_ids=true | all-gather | bytes 528384 | tf_op jit(solution)/shard_map/all_gather | solution.py:103
  96.7 0.4 fusion.18
  97.1 0.8 copy.59
  97.9 5.5 %all-to-all-start.1 = ((bf16[128,1,16]{2,1,0:T(2,128)(2,1)}), bf16[128,1,16]{2,1,0:T(2,128)(2,1)S(1)}, u32[]{:S(2)}, u32[]{:S(2)}) async-start(bf16[128,1,16]{2,1,0:T(2,128)(2,1)} %copy.59), calls=%async_computation.1 | async-start | bytes 131072 | tf_op jit(solution)/shard_map/all_to_all | solution.py:111
  104.0 8.6 %all-to-all-done.1 = bf16[128,1,16]{2,1,0:T(2,128)(2,1)S(1)} async-done(((bf16[128,1,16]{2,1,0:T(2,128)(2,1)}), bf16[128,1,16]{2,1,0:T(2,128)(2,1)S(1)}, u32[]{:S(2)}, u32[]{:S(2)}) %all-to-all-start.1) | async-done | bytes 4128 | tf_op jit(solution)/shard_map/all_to_all | solution.py:111
  112.9 0.6 multiply_reduce_fusion.1
  114.7 2.4 %copy.60 = bf16[128,1,2049]{2,1,0:T(2,128)(2,1)} copy(bf16[128,1,2049]{0,2,1:T(8,128)(2,1)S(1)} %pad_maximum_fusion) | data formatting | bytes 1049088 | tf_op jit(solution)/shard_map/concatenate | solution.py:17
  117.0 5.0 %all-to-all-start.2 = ((bf16[128,1,2049]{2,1,0:T(2,128)(2,1)}), bf16[128,1,2049]{2,1,0:T(2,128)(2,1)S(1)}, u32[]{:S(2)}, u32[]{:S(2)}) async-start(bf16[128,1,2049]{2,1,0:T(2,128)(2,1)} %copy.60), calls=%async_computation.2 | async-start | bytes 2228224 | tf_op jit(solution)/shard_map/all_to_all | solution.py:20
  122.2 19.5 %all-to-all-done.2 = bf16[128,1,2049]{2,1,0:T(2,128)(2,1)S(1)} async-done(((bf16[128,1,2049]{2,1,0:T(2,128)(2,1)}), bf16[128,1,2049]{2,1,0:T(2,128)(2,1)S(1)}, u32[]{:S(2)}, u32[]{:S(2)}) %all-to-all-start.2) | async-done | bytes 524576 | tf_op jit(solution)/shard_map/all_to_all | solution.py:20
  141.7 2.4 %compare_reduce_fusion = (pred[128]{0:T(512)(128)(4,1)S(1)}, s32[128,1,1]{2,1,0:T(1,128)S(1)}) fusion(bf16[128,1,2049]{2,1,0:T(2,128)(2,1)S(1)} %all-to-all-done.2), kind=kLoop, calls=%fused_computation.41 | loop fusion | flops 384 | bytes 896 | tf_op jit(solution)/shard_map/gt | solution.py:122
  144.4 1.1 split.9
  145.5 0.4 convolution_convert_fusion.1
  145.9 2.8 %fusion.4 = f32[4,1024]{1,0:T(4,128)S(1)} fusion(bf16[4,2048]{1,0:T(4,128)(2,1)S(1)} %convolution_convert_fusion.1, bf16[1,2048,1024]{2,1,0:T(8,128)(2,1)} %param.35), kind=kOutput, calls=%fused_computation.5 | convolution fusion | flops 16777216 | bytes 4227072 | tf_op jit(solution)/shard_map/dot_general | solution.py:32
  148.7 4.7 %fusion.9 = bf16[4,2048]{1,0:T(4,128)(2,1)S(1)} fusion(bf16[1,1024,2048]{2,1,0:T(8,128)(2,1)} %param.37, bf16[4,2048]{1,0:T(4,128)(2,1)S(1)} %convolution_convert_fusion.1, bf16[1,2048,1024]{2,1,0:T(8,128)(2,1)} %param.36, f32[4,1024]{1,0:T(4,128)S(1)} %fusion.4), kind=kOutput, calls=%fused_computation.12 | convolution fusion | flops 33587200 | bytes 8437760 | tf_op jit(solution)/shard_map/dot_general | solution.py:35
  153.8 0.5 broadcast.318
  154.3 1.0 reduce.34
  155.3 1.2 reshape.612
  156.4 4.6 %all-to-all-start.3 = ((bf16[128,2,1024]{2,1,0:T(2,128)(2,1)}), bf16[128,2,1024]{2,1,0:T(2,128)(2,1)S(1)}, u32[]{:S(2)}, u32[]{:S(2)}) async-start(bf16[128,2,1024]{2,1,0:T(2,128)(2,1)} %reshape.612), calls=%async_computation.3 | async-start | bytes 1048576 | tf_op jit(solution)/shard_map/all_to_all | solution.py:126
  161.3 4.7 %multiply_add_fusion = f32[1,4,512,512]{3,2,1,0:T(8,128)} fusion(f32[1,4,512,512]{3,2,1,0:T(8,128)} %param.30, f32[4,512]{1,0:T(4,128)S(1)} %mul.289, f32[4,512]{1,0:T(4,128)S(1)} %get-tuple-element.15, f32[4]{0:T(128)S(1)} %fusion.66), kind=kLoop, calls=%fused_computation.9 | loop fusion | flops 3145728 | bytes 8405008 | tf_op jit(solution)/shard_map/add | solution.py:98
  166.0 8.6 %all-to-all-done.3 = bf16[128,2,1024]{2,1,0:T(2,128)(2,1)S(1)} async-done(((bf16[128,2,1024]{2,1,0:T(2,128)(2,1)}), bf16[128,2,1024]{2,1,0:T(2,128)(2,1)S(1)}, u32[]{:S(2)}, u32[]{:S(2)}) %all-to-all-start.3) | async-done | bytes 524320 | tf_op jit(solution)/shard_map/all_to_all | solution.py:126
  174.6 0.4 reshape.613
  175.3 0.6 gather_fusion
  176.1 0.6 add_convert_fusion
  (68 shorter events, 3.4 us)
Async XLA Ops:
  0.6 96.1 %copy-start = (bf16[2048,16]{0,1:T(8,128)(2,1)S(1)}, bf16[2048,16]{0,1:T(8,128)(2,1)}, u32[]{:S(2)}) copy-start(bf16[2048,16]{0,1:T(8,128)(2,1)} %param.33) | copy-start | bytes 196612
  0.7 48.3 %copy-start.1 = (bf16[1,2048]{1,0:T(2,128)(2,1)S(1)}, bf16[1,2048]{1,0:T(2,128)(2,1)}, u32[]{:S(2)}) copy-start(bf16[1,2048]{1,0:T(2,128)(2,1)} %param.21) | copy-start | bytes 12292
  0.7 40.2 %copy-start.2 = (f32[2048]{0:T(1024)S(1)}, f32[2048]{0:T(1024)}, u32[]{:S(2)}) copy-start(f32[2048]{0:T(1024)} %param.22) | copy-start | bytes 24580
  0.7 40.2 %copy-start.6 = (bf16[2048,16]{0,1:T(8,128)(2,1)S(1)}, bf16[2048,16]{0,1:T(8,128)(2,1)}, u32[]{:S(2)}) copy-start(bf16[2048,16]{0,1:T(8,128)(2,1)} %param.26) | copy-start | bytes 196612
  0.7 40.2 %copy-start.7 = (bf16[2048,16]{0,1:T(8,128)(2,1)S(1)}, bf16[2048,16]{0,1:T(8,128)(2,1)}, u32[]{:S(2)}) copy-start(bf16[2048,16]{0,1:T(8,128)(2,1)} %param.25) | copy-start | bytes 196612
  0.7 40.2 %copy-start.8 = (bf16[2048,16]{0,1:T(8,128)(2,1)S(1)}, bf16[2048,16]{0,1:T(8,128)(2,1)}, u32[]{:S(2)}) copy-start(bf16[2048,16]{0,1:T(8,128)(2,1)} %param.24) | copy-start | bytes 196612
  0.7 40.2 %copy-start.9 = (bf16[2048,16]{0,1:T(8,128)(2,1)S(1)}, bf16[2048,16]{0,1:T(8,128)(2,1)}, u32[]{:S(2)}) copy-start(bf16[2048,16]{0,1:T(8,128)(2,1)} %param.23) | copy-start | bytes 196612
  0.7 50.2 %copy-start.12 = (f32[1,4]{1,0:T(1,128)S(1)}, f32[1,4]{1,0:T(1,128)}, u32[]{:S(2)}) copy-start(f32[1,4]{1,0:T(1,128)} %param.32) | copy-start | bytes 52
  0.7 50.2 %copy-start.13 = (f32[4]{0:T(128)S(1)}, f32[4]{0:T(128)}, u32[]{:S(2)}) copy-start(f32[4]{0:T(128)} %param.29) | copy-start | bytes 52
  0.7 50.2 %copy-start.10 = (bf16[2048,4]{0,1:T(4,128)(2,1)S(1)}, bf16[2048,4]{0,1:T(4,128)(2,1)}, u32[]{:S(2)}) copy-start(bf16[2048,4]{0,1:T(4,128)(2,1)} %param.28) | copy-start | bytes 49156
  0.7 50.3 %copy-start.11 = (bf16[2048,4]{0,1:T(4,128)(2,1)S(1)}, bf16[2048,4]{0,1:T(4,128)(2,1)}, u32[]{:S(2)}) copy-start(bf16[2048,4]{0,1:T(4,128)(2,1)} %param.27) | copy-start | bytes 49156
  0.8 50.5 %copy-start.14 = (s32[1,2]{1,0:T(1,128)S(1)}, s32[1,2]{1,0:T(1,128)}, u32[]{:S(2)}) copy-start(s32[1,2]{1,0:T(1,128)} %param.39) | copy-start | bytes 28
  40.5 21.0 %copy-start.3 = (f32[1,4,512]{2,1,0:T(4,128)S(1)}, f32[1,4,512]{2,1,0:T(4,128)}, u32[]{:S(2)}) copy-start(f32[1,4,512]{2,1,0:T(4,128)} %param.31) | copy-start | bytes 24580
  41.4 72.8 %copy-start.4 = (f32[2048]{0:T(1024)S(1)}, f32[2048]{0:T(1024)}, u32[]{:S(2)}) copy-start(f32[2048]{0:T(1024)} %param.34) | copy-start | bytes 24580
  42.2 16.1 %all-to-all-start = ((bf16[128,4,16]{2,1,0:T(4,128)(2,1)}), bf16[128,4,16]{2,1,0:T(4,128)(2,1)S(1)}, u32[]{:S(2)}, u32[]{:S(2)}) async-start(bf16[128,4,16]{2,1,0:T(4,128)(2,1)} %copy.57), calls=%async_computation | async-start | bytes 262144 | tf_op jit(solution)/shard_map/all_to_all | solution.py:73
  51.2 63.5 %copy-start.5 = (f32[1,4]{1,0:T(1,128)}, f32[1,4]{1,0:T(1,128)S(1)}, u32[]{:S(2)}) copy-start(f32[1,4]{1,0:T(1,128)S(1)} %get-tuple-element.11) | copy-start | bytes 52
  61.5 60.7 %copy-start.15 = (f32[1,2]{1,0:T(1,128)S(1)}, f32[1,2]{1,0:T(1,128)}, u32[]{:S(2)}) copy-start(f32[1,2]{1,0:T(1,128)} %param.41) | copy-start | bytes 28
  97.9 14.8 %all-to-all-start.1 = ((bf16[128,1,16]{2,1,0:T(2,128)(2,1)}), bf16[128,1,16]{2,1,0:T(2,128)(2,1)S(1)}, u32[]{:S(2)}, u32[]{:S(2)}) async-start(bf16[128,1,16]{2,1,0:T(2,128)(2,1)} %copy.59), calls=%async_computation.1 | async-start | bytes 131072 | tf_op jit(solution)/shard_map/all_to_all | solution.py:111
  117.0 24.6 %all-to-all-start.2 = ((bf16[128,1,2049]{2,1,0:T(2,128)(2,1)}), bf16[128,1,2049]{2,1,0:T(2,128)(2,1)S(1)}, u32[]{:S(2)}, u32[]{:S(2)}) async-start(bf16[128,1,2049]{2,1,0:T(2,128)(2,1)} %copy.60), calls=%async_computation.2 | async-start | bytes 2228224 | tf_op jit(solution)/shard_map/all_to_all | solution.py:20
  156.4 18.1 %all-to-all-start.3 = ((bf16[128,2,1024]{2,1,0:T(2,128)(2,1)}), bf16[128,2,1024]{2,1,0:T(2,128)(2,1)S(1)}, u32[]{:S(2)}, u32[]{:S(2)}) async-start(bf16[128,2,1024]{2,1,0:T(2,128)(2,1)} %reshape.612), calls=%async_computation.3 | async-start | bytes 1048576 | tf_op jit(solution)/shard_map/all_to_all | solution.py:126
where the time goes:
time: 178 us; the launch traced here: 177 us
  blocking collectives  72.8 us (41%)
  waiting for transfers between devices  43.6 us (24%)
  starting transfers between devices  21.8 us (12%)
  other arithmetic  13.8 us (8%)
  matrix products  12.3 us (7%)
  local copies, waits for them, and re-layouts  8.57 us (5%)
  between operations  3.74 us (2%)
    all_gather x1, blocking collectives, local(): piece = lax.all_gather(tokens, 'ep', axis=0, tiled=True)  38.6 us
    all_gather x1, blocking collectives, local(): lax.all_gather(gated, 'ep', axis=0, tiled=True)  34.2 us
    all_to_all x1, waiting for transfers between devices, sent_together(): lax.all_to_all(both, axis, split_axis=split_dim, concat_axis=concat_dim,...  19.5 us
    all_to_all x1, waiting for transfers between devices, local(): lax.all_to_all(proj_cols, 'ep', split_axis=0, concat_axis=1, tiled=True)  8.59 us
    all_to_all x1, waiting for transfers between devices, local(): lax.all_to_all(back_rows.reshape(devices, local_rows, width), 'ep', split...  8.57 us
    all_to_all x1, waiting for transfers between devices, local(): lax.all_to_all(result, 'ep', split_axis=0, concat_axis=2, tiled=True)  6.96 us
    all_to_all x1, starting transfers between devices, local(): lax.all_to_all(result, 'ep', split_axis=0, concat_axis=2, tiled=True)  6.71 us
    all_to_all x1, starting transfers between devices, local(): lax.all_to_all(proj_cols, 'ep', split_axis=0, concat_axis=1, tiled=True)  5.52 us
  transfers between devices with their start and end apart: 4, of which 4 were waited for; matrix products, arithmetic and copies ran while one was open for 3% of the time, Pallas kernels for 0%

commit v1 on v0

v1 whole, which is shorter than its diff:
```python
import functools

import jax
import jax.numpy as jnp
from jax import lax
from jax.experimental import pallas as pl
from jax.experimental.pallas import tpu as pltpu
from jax.sharding import PartitionSpec as P

MESH = pl.DeviceIdType.MESH
F32 = jnp.float32
BF16 = jnp.bfloat16
EPS = 1e-06
CHIPS = 64
TILE = 16
LANES = 128
MEMBERS = 32


def nt(a, b):
    return lax.dot_general(a, b, (((1,), (1,)), ((), ())), preferred_element_type=F32)


def nn(a, b):
    return lax.dot_general(a, b, (((1,), (0,)), ((), ())), preferred_element_type=F32)


def tn(a, b):
    return lax.dot_general(a, b, (((0,), (0,)), ((), ())), preferred_element_type=F32)


def iota(shape, dim):
    return lax.broadcasted_iota(jnp.int32, shape, dim)


def pieces(row):
    return [row[:, LANES * s : LANES * (s + 1)] for s in range(row.shape[1] // LANES)]


def layer(
    tokens,
    mixer_gain,
    wq,
    wk,
    wv,
    wo,
    wi,
    wf,
    forget_bias,
    memory,
    memory_norm,
    memory_max,
    wm,
    expert_gain,
    gate,
    up,
    down,
    route_group,
    route_member,
    group_weight,
    member_weight,
    out_ref,
    next_memory,
    next_norm,
    next_max_ref,
    w_all,
    mem,
    mem16,
    gate_v,
    up_v,
    down_v,
    spread,
    perm,
    rows32,
    tok_rows,
    tile32,
    a_buf,
    b_src,
    b_buf,
    c_buf,
    p_buf,
    f_src,
    f_buf,
    e_rows,
    x_rows,
    r_rows,
    r_send,
    send_sem,
    recv_sem,
    load_sem,
    w_sem,
    out_sem,
    pair_sem,
):
    me = lax.axis_index("ep")
    core = lax.rem(me, 2)
    chip = lax.div(me, 2)
    other = 1 - core
    partner = me + 1 - 2 * core
    cz, cy, cx = lax.div(chip, 16), lax.rem(lax.div(chip, 4), 4), lax.rem(chip, 4)

    def peer(i):
        dz, dy, dx = lax.div(i, 16), lax.rem(lax.div(i, 4), 4), lax.rem(i, 4)
        there = lax.rem(cz + dz, 4) * 16 + lax.rem(cy + dy, 4) * 4 + lax.rem(cx + dx, 4)
        return there, there * 2 + core

    barrier = pltpu.get_barrier_semaphore()

    def greet(i, carry):
        pl.semaphore_signal(barrier, inc=1, device_id=(peer(i)[1],), device_id_type=MESH)
        return carry

    lax.fori_loop(1, CHIPS, greet, 0)
    pl.semaphore_signal(barrier, inc=1, device_id=(partner,), device_id_type=MESH)

    own_loads = []
    for j, ref in enumerate((wq, wk, wv, wo, wm)):
        own_loads.append(pltpu.make_async_copy(ref, w_all.at[j, core], w_sem.at[j]))
    mem_load = pltpu.make_async_copy(memory, mem, load_sem.at[0])
    gate_loads = [pltpu.make_async_copy(gate.at[:, u], gate_v.at[u], load_sem.at[1 + u]) for u in range(2)]
    up_loads = [pltpu.make_async_copy(up.at[:, u], up_v.at[u], load_sem.at[3 + u]) for u in range(2)]
    down_load = pltpu.make_async_copy(down, down_v, load_sem.at[5])
    for load in own_loads + [mem_load] + gate_loads + up_loads + [down_load]:
        load.start()

    def exchange(phase, source, buf):
        def send(n, carry):
            there, device = peer(CHIPS - n)
            pltpu.make_async_remote_copy(
                src_ref=source(there),
                dst_ref=buf.at[chip],
                send_sem=send_sem.at[phase],
                recv_sem=recv_sem.at[phase],
                device_id=(device,),
                device_id_type=MESH,
            ).start()
            return carry

        lax.fori_loop(1, CHIPS, send, 0)

    def whole(phase, buf):
        span = buf.at[pl.ds(0, CHIPS - 1)]
        return pltpu.make_async_remote_copy(
            src_ref=span,
            dst_ref=span,
            send_sem=send_sem.at[phase],
            recv_sem=recv_sem.at[phase],
            device_id=(partner,),
            device_id_type=MESH,
        )

    token = tokens[...].astype(F32)
    for s, piece in enumerate(pieces(token)):
        tile32[s : s + 1, :] = piece
    a_buf[chip] = tile32[...].astype(BF16)

    pl.semaphore_wait(barrier, CHIPS)

    exchange(0, lambda there: a_buf.at[chip], a_buf)
    swaps = []
    for j, ref in enumerate((wq, wk, wv, wo, wm)):
        swaps.append(
            pltpu.make_async_remote_copy(
                src_ref=ref,
                dst_ref=w_all.at[j, core],
                send_sem=pair_sem.at[0, j],
                recv_sem=pair_sem.at[1, j],
                device_id=(partner,),
                device_id_type=MESH,
            )
        )
        swaps[j].start()

    gain = mixer_gain[...]
    scale = lax.rsqrt(jnp.mean(token * token, axis=-1, keepdims=True) + EPS)
    normed = (token * scale * gain).astype(BF16).astype(F32)
    head_of = iota((4, 1), 0)

    def column(read):
        value = jnp.zeros((4, 1), F32)
        for h in range(4):
            value = jnp.where(head_of == h, read(h), value)
        return value

    input_pre = jnp.sum(wi[...].astype(F32) * normed, axis=1, keepdims=True)
    forget_pre = jnp.sum(wf[...].astype(F32) * normed, axis=1, keepdims=True) + column(lambda h: forget_bias[h])
    log_forget = jnp.minimum(forget_pre, 0.0) - jnp.log1p(jnp.exp(-jnp.abs(forget_pre)))
    held = log_forget + column(lambda h: memory_max[0, h])
    next_max = jnp.maximum(held, input_pre)
    keep = jnp.exp(held - next_max)
    admit = jnp.exp(input_pre - next_max)
    next_max_ref[...] = jnp.sum(
        jnp.where(iota((4, 4), 0) == iota((4, 4), 1), jnp.broadcast_to(next_max, (4, 4)), 0.0), axis=0, keepdims=True
    )

    lane = iota((1, LANES), 1)
    e0 = (route_group[0] * MEMBERS + route_member[0, 0]).astype(F32)
    e1 = (route_group[0] * MEMBERS + route_member[0, 1]).astype(F32)
    w0 = group_weight[0] * member_weight[0, 0]
    w1 = group_weight[0] * member_weight[0, 1]
    routing = jnp.where(lane == 0, e0, jnp.where(lane == 1, e1, jnp.where(lane == 2, w0, jnp.where(lane == 3, w1, 0.0))))
    b_src[:, 1:2, :] = jnp.broadcast_to(routing[None], (CHIPS, 1, LANES))

    for j in range(4):
        a, b = iota((LANES, 512), 0), iota((LANES, 512), 1)
        spread[:, 512 * j : 512 * (j + 1)] = (a == 32 * j + lax.rem(b, 32)).astype(F32).astype(BF16)
    a, b = iota((256, 256), 0), iota((256, 256), 1)
    perm[...] = (b == 128 * lax.rem(lax.div(a, 16), 2) + 16 * lax.div(a, 32) + lax.rem(a, 16)).astype(F32).astype(BF16)

    def reorder(rows):
        q = perm[...]
        parts = [nn(rows[:, 256 * m : 256 * (m + 1)], q) for m in range(8)]
        return jnp.concatenate([p[:, :LANES] for p in parts] + [p[:, LANES:] for p in parts], axis=1)

    def restore(rows):
        q = perm[...]
        parts = [
            nt(jnp.concatenate([rows[:, LANES * m : LANES * (m + 1)], rows[:, 1024 + LANES * m : 1024 + LANES * (m + 1)]], axis=1), q)
            for m in range(8)
        ]
        return jnp.concatenate(parts, axis=1)

    g = expert_gain[...]
    g_hi = g.astype(BF16)
    g_mid = (g - g_hi.astype(F32)).astype(BF16)
    g_lo = (g - g_hi.astype(F32) - g_mid.astype(F32)).astype(BF16)
    late_gain = jnp.zeros((1, 2048), F32)
    for part in (g_hi, g_mid, g_lo):
        late_gain = late_gain + reorder(jnp.broadcast_to(part.astype(F32), (16, 2048)).astype(BF16))[0:1]

    mem_load.wait()
    for h in range(4):
        mem16[h] = mem[h].astype(BF16)
    for load in own_loads:
        load.wait()
    for swap in swaps:
        swap.wait_recv()

    def gathered(buf):
        rows32[...] = buf[...].astype(F32).reshape(CHIPS * TILE, LANES)
        return [rows32[pl.ds(s, CHIPS, stride=TILE), :] for s in range(TILE)]

    whole(0, a_buf).wait_recv()
    parts = gathered(a_buf)
    tok_rows[...] = jnp.concatenate([p.astype(BF16) for p in parts], axis=1)
    squares = parts[0] * parts[0]
    for p in parts[1:]:
        squares = squares + p * p
    scale = lax.rsqrt(jnp.sum(squares, axis=-1, keepdims=True) * (1.0 / 2048.0) + EPS)
    normed_rows = jnp.concatenate(
        [(p * scale * gain[:, LANES * s : LANES * (s + 1)]).astype(BF16) for s, p in enumerate(parts)], axis=1
    )
    cols = nt(normed_rows, w_all[0:4].reshape(LANES, 2048)).astype(BF16).astype(F32)
    b_src[:, 0:1, :] = cols.reshape(CHIPS, 1, LANES)
    exchange(1, lambda there: b_src.at[there], b_buf)
    b_buf[chip] = b_src[chip]

    whole(1, b_buf).wait_recv()
    got = b_buf[:, 0:1, :].reshape(CHIPS, LANES).astype(BF16)
    wide = nn(got, spread[...])
    mine = lax.div(lax.rem(iota((CHIPS, 2048), 1), 512), 32) == lax.rem(iota((CHIPS, 2048), 0), 16)
    wide = jnp.where(mine, wide, 0.0).astype(BF16)
    heads = (iota((16, CHIPS), 0) == lax.div(iota((16, CHIPS), 1), 16)).astype(F32).astype(BF16)
    packed = nn(heads, wide)[0:4]
    query, key_raw, value, outgate = (packed[:, 512 * j : 512 * (j + 1)] for j in range(4))
    key = key_raw * (512.0**-0.5)
    score = jnp.sum(key * query, axis=-1, keepdims=True)
    old_norm = memory_norm[0]
    denom = keep * jnp.sum(old_norm * query, axis=-1, keepdims=True) + admit * score
    query16 = query.astype(BF16)
    head_row = iota((4, 512), 0)
    carried = jnp.zeros((4, 512), F32)
    for h in range(4):
        carried = jnp.where(head_row == h, nt(query16, mem16[h]), carried)
    numer = keep * carried + (admit * score) * value
    head_out = numer / jnp.maximum(jnp.abs(denom), jnp.exp(-next_max))
    gated = head_out * jax.nn.sigmoid(outgate)
    for b in range(4):
        tile32[pl.ds(b, 4, stride=4), :] = gated[:, LANES * b : LANES * (b + 1)]
    c_buf[chip] = tile32[...].astype(BF16)
    exchange(2, lambda there: c_buf.at[chip], c_buf)

    next_norm[0] = keep * old_norm + admit * key
    grow = admit * (512.0**-0.5)
    value16 = value.astype(BF16)
    stores = []
    for h in range(4):
        pick = jnp.where(head_row == h, key_raw, 0.0).astype(BF16)
        outer = tn(value16, pick)
        mem[h] = keep[h : h + 1] * mem[h] + grow[h : h + 1] * outer
        stores.append(pltpu.make_async_copy(mem.at[h], next_memory.at[h], out_sem.at[h]))
        stores[h].start()

    table = b_buf[:, 1:2, :].reshape(CHIPS, LANES)
    t0, t1, u0, u1 = (table[:, k : k + 1] for k in range(4))
    below = (iota((CHIPS, CHIPS), 0) > iota((CHIPS, CHIPS), 1)).astype(F32).astype(BF16)
    slot = iota((CHIPS, LANES), 1)
    choose = jnp.where((slot == 4) & (iota((CHIPS, LANES), 0) == chip), 1.0, 0.0)
    weigh = jnp.zeros((CHIPS, LANES), F32)
    for k in range(2):
        eid = (2 * chip + k).astype(F32)
        first, second = t0 == eid, t1 == eid
        hit = jnp.where(first | second, 1.0, 0.0)
        rank = nn(below, jnp.broadcast_to(hit, (CHIPS, LANES)).astype(BF16))
        here = (rank == (slot - 8 * k).astype(F32)) & (slot >= 8 * k) & (slot < 8 * k + 4)
        taken = jnp.where(here, hit, 0.0)
        choose = choose + taken
        weigh = weigh + taken * (jnp.where(first, u0, 0.0) + jnp.where(second, u1, 0.0))
    select = jnp.concatenate([choose, choose], axis=0).T[0:16]
    both = jnp.concatenate(
        [jnp.where(lane < CHIPS, select, 0.0), jnp.where(lane < CHIPS, 0.0, select)], axis=0
    ).astype(BF16)
    slot_tokens = reorder(nn(select[:, :CHIPS].astype(BF16), tok_rows[...]).astype(BF16))
    weigh = weigh[:, :16]
    weigh_hi = weigh.astype(BF16)
    weigh_lo = (weigh - weigh_hi.astype(F32)).astype(BF16)

    whole(2, c_buf).wait_recv()
    rows = jnp.concatenate([p.astype(BF16) for p in gathered(c_buf)], axis=1)
    flat = nt(w_all[4].reshape(32, 2048), jnp.concatenate([rows, rows], axis=0))
    p_buf[chip] = jnp.where(lane < CHIPS, flat[0:16], flat[16:32]).astype(BF16)
    exchange(3, lambda there: p_buf.at[chip], p_buf)

    whole(3, p_buf).wait_recv()
    halves = nt(both, p_buf[...].reshape(CHIPS * TILE, LANES))
    projected = jnp.concatenate([halves[0:16], halves[16:32]], axis=1)
    middle = (slot_tokens + projected).astype(BF16)
    middle32 = middle.astype(F32)
    scale = lax.rsqrt(jnp.mean(middle32 * middle32, axis=-1, keepdims=True) + EPS)
    expert_in = (middle32 * scale * late_gain).astype(BF16).astype(F32)
    e_rows[0] = expert_in[0:8]
    e_rows[1] = expert_in[8:16]

    def to_partner(n, source, target):
        return pltpu.make_async_remote_copy(
            src_ref=source,
            dst_ref=target,
            send_sem=pair_sem.at[0, n],
            recv_sem=pair_sem.at[1, n],
            device_id=(partner,),
            device_id_type=MESH,
        )

    rows_over = to_partner(5, e_rows.at[other], x_rows.at[core])
    rows_over.start()
    x_rows[core] = e_rows[core]
    for load in gate_loads + up_loads + [down_load]:
        load.wait()
    rows_over.wait_recv()
    x = x_rows[...].reshape(16, 2048).astype(BF16)
    result = jnp.zeros((16, 2048), F32)
    for n in range(4):
        span = slice(256 * n, 256 * (n + 1))
        gate_part = nn(x[:, :1024], gate_v[0, :, :, span].reshape(1024, 256)) + nn(
            x[:, 1024:], gate_v[1, :, :, span].reshape(1024, 256)
        )
        up_part = nn(x[:, :1024], up_v[0, :, :, span].reshape(1024, 256)) + nn(
            x[:, 1024:], up_v[1, :, :, span].reshape(1024, 256)
        )
        hidden = (gate_part / (1.0 + jnp.exp(-gate_part)) * up_part).astype(BF16)
        result = result + nn(hidden, down_v[span, :])
    result = result.astype(BF16).astype(F32)
    r_send[0] = result[0:8]
    r_send[1] = result[8:16]
    rows_back = to_partner(6, r_send.at[other], r_rows.at[core])
    rows_back.start()
    r_rows[core] = r_send[core]
    own_middle = restore(middle)[4:5]
    for s, piece in enumerate(pieces(own_middle)):
        tile32[s : s + 1, :] = piece
    rows_back.wait_recv()

    slots = r_rows[...].reshape(16, 2048).astype(BF16)
    mixed = nn(weigh_hi, slots) + nn(weigh_lo, slots)
    for s, piece in enumerate(pieces(mixed)):
        rows32[pl.ds(s, CHIPS, stride=TILE), :] = piece
    f_src[...] = rows32[...].reshape(CHIPS, TILE, LANES).astype(BF16)
    exchange(4, lambda there: f_src.at[there], f_buf)
    f_buf[chip] = f_src[chip]
    whole(4, f_buf).wait_recv()
    total = tile32[...] + jnp.sum(f_buf[...].astype(F32), axis=0)
    final = total.astype(BF16).astype(F32)
    for s in range(TILE):
        out_ref[:, LANES * s : LANES * (s + 1)] = final[s : s + 1].astype(BF16)

    for phase, buf in enumerate((a_buf, b_buf, c_buf, p_buf, f_buf)):
        whole(phase, buf).wait_send()
    for swap in swaps:
        swap.wait_send()
    rows_over.wait_send()
    rows_back.wait_send()
    for store in stores:
        store.wait()


def local(
    tokens,
    mixer_gain,
    query_weight,
    key_weight,
    value_weight,
    outgate_weight,
    input_weight,
    forget_weight,
    forget_bias,
    memory_matrix,
    memory_norm,
    memory_max,
    mixer_out,
    expert_gain,
    expert_gate,
    expert_up,
    expert_down,
    route_group,
    route_member,
    group_weight,
    member_weight,
):
    vmem = pl.BlockSpec(memory_space=pltpu.VMEM)
    smem = pl.BlockSpec(memory_space=pltpu.SMEM)
    hbm = pl.BlockSpec(memory_space=pl.ANY)
    dma = pltpu.SemaphoreType.DMA
    out, matrix, norm, top = pl.pallas_call(
        layer,
        out_shape=(
            jax.ShapeDtypeStruct((1, 2048), BF16),
            jax.ShapeDtypeStruct((4, 512, 512), F32),
            jax.ShapeDtypeStruct((1, 4, 512), F32),
            jax.ShapeDtypeStruct((1, 4), F32),
        ),
        in_specs=[vmem, vmem, hbm, hbm, hbm, hbm, vmem, vmem, smem, hbm, vmem, smem, hbm, vmem, hbm, hbm, hbm, smem, smem, smem, smem],
        out_specs=(vmem, hbm, vmem, vmem),
        scratch_shapes=[
            pltpu.VMEM((5, 2, 16, 2048), BF16),
            pltpu.VMEM((4, 512, 512), F32),
            pltpu.VMEM((4, 512, 512), BF16),
            pltpu.VMEM((2, CHIPS, 16, 1024), BF16),
            pltpu.VMEM((2, CHIPS, 16, 1024), BF16),
            pltpu.VMEM((1024, 2048), BF16),
            pltpu.VMEM((LANES, 2048), BF16),
            pltpu.VMEM((256, 256), BF16),
            pltpu.VMEM((CHIPS * TILE, LANES), F32),
            pltpu.VMEM((CHIPS, 2048), BF16),
            pltpu.VMEM((TILE, LANES), F32),
            pltpu.VMEM((CHIPS, TILE, LANES), BF16),
            pltpu.VMEM((CHIPS, 2, LANES), F32),
            pltpu.VMEM((CHIPS, 2, LANES), F32),
            pltpu.VMEM((CHIPS, TILE, LANES), BF16),
            pltpu.VMEM((CHIPS, TILE, LANES), BF16),
            pltpu.VMEM((CHIPS, TILE, LANES), BF16),
            pltpu.VMEM((CHIPS, TILE, LANES), BF16),
            pltpu.VMEM((2, 8, 2048), F32),
            pltpu.VMEM((2, 8, 2048), F32),
            pltpu.VMEM((2, 8, 2048), F32),
            pltpu.VMEM((2, 8, 2048), F32),
            dma((5,)),
            dma((5,)),
            dma((6,)),
            dma((5,)),
            dma((4,)),
            dma((2, 7)),
        ],
        compiler_params=pltpu.CompilerParams(collective_id=0, has_side_effects=True),
    )(
        tokens,
        mixer_gain.reshape(1, 2048),
        query_weight.T,
        key_weight.T,
        value_weight.T,
        outgate_weight.T,
        input_weight.T,
        forget_weight.T,
        forget_bias,
        memory_matrix.reshape(4, 512, 512),
        memory_norm,
        memory_max,
        mixer_out.T,
        expert_gain.reshape(1, 2048),
        expert_gate.reshape(CHIPS, 2, 16, 1024),
        expert_up.reshape(CHIPS, 2, 16, 1024),
        expert_down.reshape(1024, 2048),
        route_group,
        route_member,
        group_weight,
        member_weight,
    )
    return out, matrix.reshape(1, 4, 512, 512), norm, top


def solution(mesh):
    columns, rows = P(None, "ep"), P("ep", None)
    cube, block = P("ep", None, None), P("ep", None, None, None)
    placed = (
        rows, P(), columns, columns, columns, columns, P(), P(), P(), block, cube, rows, columns, P(), cube, cube, cube,
        P("ep"), rows, P("ep"), rows,
    )
    return jax.shard_map(local, mesh=mesh, in_specs=placed, out_specs=(rows, block, cube, rows), check_vma=False)
```

time: 178 us -> 60 us (0.34)
  blocking collectives: 72.8 us -> 0 us
  Pallas kernels: 0 us -> 50.8 us
  waiting for transfers between devices: 43.6 us -> 0 us
  starting transfers between devices: 21.8 us -> 0 us
  other arithmetic: 13.8 us -> 0 us
  matrix products: 12.3 us -> 0 us
  between operations: 3.74 us -> 1.94 us
    all_gather x2 -> x0, blocking collectives: 72.8 us -> none  [the longest x1 38.6 us: local(): piece = lax.all_gather(tokens, 'ep', axis=0, tiled=True)]
    pallas_call x0 -> x1, Pallas kernels: none -> 50.8 us  [local(): pl.pallas_call(layer, out_shape=(jax.ShapeDtypeStruct((1, 2048), BF16), j...]
    all_to_all x4 -> x0, waiting for transfers between devices: 43.6 us -> none  [the longest x1 19.5 us: sent_together(): lax.all_to_all(both, axis, split_axis=split_dim, concat_axis=concat_dim,...]
    all_to_all x4 -> x0, starting transfers between devices: 21.8 us -> none  [the longest x1 6.71 us: local(): lax.all_to_all(result, 'ep', split_axis=0, concat_axis=2, tiled=True)]
    dot_general x9 -> x0, matrix products: 12.3 us -> none  [the longest x1 4.67 us: run_expert(): jnp.dot(hidden, down_mat, preferred_element_type=jnp.float32)]
    unnamed x36 -> x8, local copies, waits for them, and re-layouts: 1.78 us -> 7.07 us
    add x2 -> x0, other arithmetic: 4.74 us -> none  [the longest x1 4.74 us: local(): keep[..., None, None] * memory_matrix]
    reduce_sum x5 -> x0, other arithmetic: 2.53 us -> none  [the longest x3 1.61 us: root_norm(): jnp.mean(values * values, axis=-1, keepdims=True) + norm_eps]
  transfers between devices with their start and end apart: 4 -> 0, of which waited for: 4 -> 0; matrix products, arithmetic and copies ran while one was open for 3% -> 0% of each run, Pallas kernels for 0% -> 0%
where the time goes in v1:
time: 60 us; the launch traced here: 59.8 us
  Pallas kernels  50.8 us (85%)
  local copies, waits for them, and re-layouts  7.07 us (12%)
  between operations  1.94 us (3%)
    pallas_call x1, Pallas kernels, local(): pl.pallas_call(layer, out_shape=(jax.ShapeDtypeStruct((1, 2048), BF16), j...  50.8 us
    unnamed x8, local copies, waits for them, and re-layouts  7.07 us

profile of v1, /device:TPU:0, one launch (start us, length us, event | category | flops | bytes accessed | tf_op | source)
XLA Modules:
  0.0 59.8 jit_solution(10037162871894907426)
XLA Ops:
  1.9 50.8 %shard_map.228 = (bf16[1,2048]{1,0:T(2,128)(2,1)}, f32[4,512,512]{2,1,0:T(8,128)}, f32[1,4,512]{2,1,0:T(4,128)}, f32[1,4]{1,0:T(1,128)}) custom-call(bf16[1,2048]{1,0:T(2,128)(2,1)} %tokens.1, f32[1,2048]{1,0:T(1,128)} %bitcast.26, bf16[16,2048]{1,0:T(8,128)(2,1)} %bitcast.19, bf16[16,2048]{1,0:T(8,128)(2,1)} %bitcast.20, bf16[16,2048]{1,0:T(8,128)(2,1)} %bitcast.21, ...), custom_call_target="tpu_custom_call" | custom-call | tf_op jit(solution)/shard_map/pallas_call | solution.py:423
  52.7 1.3 %copy.31 = bf16[1,2048]{1,0:T(2,128)(2,1)} copy(bf16[1,2048]{1,0:T(2,128)(2,1)} %get-tuple-element.16) | data formatting | bytes 8192
  54.0 0.0 copy-start
  54.0 0.0 copy-start.1
  54.0 4.7 %copy.32 = f32[1,4,512,512]{3,2,1,0:T(8,128)} copy(f32[1,4,512,512]{3,2,1,0:T(8,128)} %bitcast.18) | data formatting | bytes 8388608
  58.7 0.0 copy-done
  58.7 0.6 %copy.33 = f32[1,4,512]{2,1,0:T(4,128)} copy(f32[1,4,512]{2,1,0:T(4,128)S(1)} %copy-done) | data formatting | bytes 16384
  59.3 0.0 copy-done.1
  59.3 0.5 copy.34
Async XLA Ops:
  54.0 4.7 %copy-start = (f32[1,4,512]{2,1,0:T(4,128)S(1)}, f32[1,4,512]{2,1,0:T(4,128)}, u32[]{:S(2)}) copy-start(f32[1,4,512]{2,1,0:T(4,128)} %get-tuple-element.18) | copy-start | bytes 24580
  54.0 5.3 %copy-start.1 = (f32[1,4]{1,0:T(1,128)S(1)}, f32[1,4]{1,0:T(1,128)}, u32[]{:S(2)}) copy-start(f32[1,4]{1,0:T(1,128)} %get-tuple-element.19) | copy-start | bytes 52

commit v2 on v1

--- a/solution.py
+++ b/solution.py
@@ -38,39 +38,48 @@
 
 
 def layer(
-    tokens,
-    mixer_gain,
+    tokens_in,
+    mixer_gain_in,
     wq,
     wk,
     wv,
     wo,
-    wi,
-    wf,
-    forget_bias,
+    wi_in,
+    wf_in,
+    forget_bias_in,
     memory,
-    memory_norm,
-    memory_max,
+    memory_norm_in,
+    memory_max_in,
     wm,
-    expert_gain,
+    expert_gain_in,
     gate,
     up,
     down,
+    route_member_in,
+    member_weight_in,
     route_group,
-    route_member,
     group_weight,
-    member_weight,
     out_ref,
-    next_memory,
+    mem,
     next_norm,
     next_max_ref,
+    tokens,
+    mixer_gain,
+    wi,
+    wf,
+    memory_norm,
+    expert_gain,
+    forget_bias,
+    memory_max,
+    route_member,
+    member_weight,
     w_all,
-    mem,
+    w_mix,
     mem16,
     gate_v,
     up_v,
     down_v,
     spread,
-    perm,
     rows32,
     tok_rows,
     tile32,
@@ -88,9 +97,10 @@
     send_sem,
     recv_sem,
     load_sem,
+    small_sem,
     w_sem,
-    out_sem,
     pair_sem,
+    line_sem,
 ):
     me = lax.axis_index("ep")
     core = lax.rem(me, 2)
@@ -113,22 +123,36 @@
     lax.fori_loop(1, CHIPS, greet, 0)
     pl.semaphore_signal(barrier, inc=1, device_id=(partner,), device_id_type=MESH)
 
-    own_loads = []
-    for j, ref in enumerate((wq, wk, wv, wo, wm)):
-        own_loads.append(pltpu.make_async_copy(ref, w_all.at[j, core], w_sem.at[j]))
+    small = (
+        (tokens_in, tokens),
+        (mixer_gain_in, mixer_gain),
+        (wi_in, wi),
+        (wf_in, wf),
+        (memory_norm_in, memory_norm),
+        (expert_gain_in, expert_gain),
+        (forget_bias_in, forget_bias),
+        (memory_max_in, memory_max),
+        (route_member_in, route_member),
+        (member_weight_in, member_weight),
+    )
+    small_loads = [pltpu.make_async_copy(ref, into, small_sem.at[n]) for n, (ref, into) in enumerate(small)]
+    own_loads = [
+        pltpu.make_async_copy(ref, w_all.at[j, core], w_sem.at[j]) for j, ref in enumerate((wq, wk, wv, wo))
+    ] + [pltpu.make_async_copy(wm, w_mix.at[cx, core], w_sem.at[4])]
     mem_load = pltpu.make_async_copy(memory, mem, load_sem.at[0])
-    gate_loads = [pltpu.make_async_copy(gate.at[:, u], gate_v.at[u], load_sem.at[1 + u]) for u in range(2)]
-    up_loads = [pltpu.make_async_copy(up.at[:, u], up_v.at[u], load_sem.at[3 + u]) for u in range(2)]
-    down_load = pltpu.make_async_copy(down, down_v, load_sem.at[5])
-    for load in own_loads + [mem_load] + gate_loads + up_loads + [down_load]:
+    expert_loads = [
+        pltpu.make_async_copy(ref, into, load_sem.at[1 + n])
+        for n, (ref, into) in enumerate(((gate, gate_v), (up, up_v), (down, down_v)))
+    ]
+    for load in small_loads + own_loads + [mem_load] + expert_loads:
         load.start()
 
-    def exchange(phase, source, buf):
+    def exchange(phase, source, buf, stride=1, slot=chip):
         def send(n, carry):
-            there, device = peer(CHIPS - n)
+            there, device = peer(CHIPS - stride * n)
             pltpu.make_async_remote_copy(
                 src_ref=source(there),
-                dst_ref=buf.at[chip],
+                dst_ref=buf.at[slot],
                 send_sem=send_sem.at[phase],
                 recv_sem=recv_sem.at[phase],
                 device_id=(device,),
@@ -136,10 +160,10 @@
             ).start()
             return carry
 
-        lax.fori_loop(1, CHIPS, send, 0)
+        lax.fori_loop(1, CHIPS // stride, send, 0)
 
     def whole(phase, buf):
-        span = buf.at[pl.ds(0, CHIPS - 1)]
+        span = buf.at[pl.ds(0, buf.shape[0] - 1)]
         return pltpu.make_async_remote_copy(
             src_ref=span,
             dst_ref=span,
@@ -149,6 +173,8 @@
             device_id_type=MESH,
         )
 
+    for load in small_loads:
+        load.wait()
     token = tokens[...].astype(F32)
     for s, piece in enumerate(pieces(token)):
         tile32[s : s + 1, :] = piece
@@ -162,7 +188,7 @@
         swaps.append(
             pltpu.make_async_remote_copy(
                 src_ref=ref,
-                dst_ref=w_all.at[j, core],
+                dst_ref=w_all.at[j, core] if j < 4 else w_mix.at[cx, core],
                 send_sem=pair_sem.at[0, j],
                 recv_sem=pair_sem.at[1, j],
                 device_id=(partner,),
@@ -204,41 +230,18 @@
     for j in range(4):
         a, b = iota((LANES, 512), 0), iota((LANES, 512), 1)
         spread[:, 512 * j : 512 * (j + 1)] = (a == 32 * j + lax.rem(b, 32)).astype(F32).astype(BF16)
-    a, b = iota((256, 256), 0), iota((256, 256), 1)
-    perm[...] = (b == 128 * lax.rem(lax.div(a, 16), 2) + 16 * lax.div(a, 32) + lax.rem(a, 16)).astype(F32).astype(BF16)
-
-    def reorder(rows):
-        q = perm[...]
-        parts = [nn(rows[:, 256 * m : 256 * (m + 1)], q) for m in range(8)]
-        return jnp.concatenate([p[:, :LANES] for p in parts] + [p[:, LANES:] for p in parts], axis=1)
-
-    def restore(rows):
-        q = perm[...]
-        parts = [
-            nt(jnp.concatenate([rows[:, LANES * m : LANES * (m + 1)], rows[:, 1024 + LANES * m : 1024 + LANES * (m + 1)]], axis=1), q)
-            for m in range(8)
-        ]
-        return jnp.concatenate(parts, axis=1)
-
-    g = expert_gain[...]
-    g_hi = g.astype(BF16)
-    g_mid = (g - g_hi.astype(F32)).astype(BF16)
-    g_lo = (g - g_hi.astype(F32) - g_mid.astype(F32)).astype(BF16)
-    late_gain = jnp.zeros((1, 2048), F32)
-    for part in (g_hi, g_mid, g_lo):
-        late_gain = late_gain + reorder(jnp.broadcast_to(part.astype(F32), (16, 2048)).astype(BF16))[0:1]
-
     mem_load.wait()
     for h in range(4):
         mem16[h] = mem[h].astype(BF16)
     for load in own_loads:
         load.wait()
-    for swap in swaps:
+    for swap in swaps[:4]:
         swap.wait_recv()
 
     def gathered(buf):
-        rows32[...] = buf[...].astype(F32).reshape(CHIPS * TILE, LANES)
-        return [rows32[pl.ds(s, CHIPS, stride=TILE), :] for s in range(TILE)]
+        count = buf.shape[0]
+        rows32[0 : count * TILE, :] = buf[...].astype(F32).reshape(count * TILE, LANES)
+        return [rows32[pl.ds(s, count, stride=TILE), :] for s in range(TILE)]
 
     whole(0, a_buf).wait_recv()
     parts = gathered(a_buf)
@@ -250,10 +253,23 @@
     normed_rows = jnp.concatenate(
         [(p * scale * gain[:, LANES * s : LANES * (s + 1)]).astype(BF16) for s, p in enumerate(parts)], axis=1
     )
-    cols = nt(normed_rows, w_all[0:4].reshape(LANES, 2048)).astype(BF16).astype(F32)
+    cols = nt(normed_rows, w_all[...].reshape(LANES, 2048)).astype(BF16).astype(F32)
     b_src[:, 0:1, :] = cols.reshape(CHIPS, 1, LANES)
     exchange(1, lambda there: b_src.at[there], b_buf)
     b_buf[chip] = b_src[chip]
+    line_sends = [
+        pltpu.make_async_remote_copy(
+            src_ref=w_mix.at[cx, core],
+            dst_ref=w_mix.at[cx, core],
+            send_sem=line_sem.at[0, d - 1],
+            recv_sem=line_sem.at[1, d - 1],
+            device_id=(((chip - cx + lax.rem(cx + d, 4)) * 2 + core),),
+            device_id_type=MESH,
+        )
+        for d in (2, 1, 3)
+    ]
+    for copy in line_sends:
+        copy.start()
 
     whole(1, b_buf).wait_recv()
     got = b_buf[:, 0:1, :].reshape(CHIPS, LANES).astype(BF16)
@@ -277,19 +293,34 @@
     gated = head_out * jax.nn.sigmoid(outgate)
     for b in range(4):
         tile32[pl.ds(b, 4, stride=4), :] = gated[:, LANES * b : LANES * (b + 1)]
-    c_buf[chip] = tile32[...].astype(BF16)
-    exchange(2, lambda there: c_buf.at[chip], c_buf)
+    spot = lax.div(chip, 4)
+    c_buf[spot] = tile32[...].astype(BF16)
+    exchange(2, lambda there: c_buf.at[spot], c_buf, 4, spot)
+
+    line_shares = []
+    for n, copy in enumerate(line_sends):
+        copy.wait_recv()
+    for n in range(3):
+        block = w_mix.at[lax.rem(cx + n + 1, 4), core]
+        line_shares.append(
+            pltpu.make_async_remote_copy(
+                src_ref=block,
+                dst_ref=block,
+                send_sem=line_sem.at[2, n],
+                recv_sem=line_sem.at[3, n],
+                device_id=(partner,),
+                device_id_type=MESH,
+            )
+        )
+        line_shares[n].start()
 
     next_norm[0] = keep * old_norm + admit * key
     grow = admit * (512.0**-0.5)
     value16 = value.astype(BF16)
-    stores = []
     for h in range(4):
         pick = jnp.where(head_row == h, key_raw, 0.0).astype(BF16)
         outer = tn(value16, pick)
         mem[h] = keep[h : h + 1] * mem[h] + grow[h : h + 1] * outer
-        stores.append(pltpu.make_async_copy(mem.at[h], next_memory.at[h], out_sem.at[h]))
-        stores[h].start()
 
     table = b_buf[:, 1:2, :].reshape(CHIPS, LANES)
     t0, t1, u0, u1 = (table[:, k : k + 1] for k in range(4))
@@ -306,28 +337,30 @@
         taken = jnp.where(here, hit, 0.0)
         choose = choose + taken
         weigh = weigh + taken * (jnp.where(first, u0, 0.0) + jnp.where(second, u1, 0.0))
-    select = jnp.concatenate([choose, choose], axis=0).T[0:16]
-    both = jnp.concatenate(
-        [jnp.where(lane < CHIPS, select, 0.0), jnp.where(lane < CHIPS, 0.0, select)], axis=0
-    ).astype(BF16)
-    slot_tokens = reorder(nn(select[:, :CHIPS].astype(BF16), tok_rows[...]).astype(BF16))
+    select = jnp.concatenate([choose, choose], axis=0).T[0:16, 0:CHIPS].astype(BF16)
+    slot_tokens = nn(select, tok_rows[...])
+    a, b = iota((CHIPS, CHIPS), 0), iota((CHIPS, CHIPS), 1)
+    by_line = (b == lax.rem(a, 4) * 16 + lax.div(a, 4)).astype(F32).astype(BF16)
+    select_line = nn(select, by_line).astype(BF16)
     weigh = weigh[:, :16]
     weigh_hi = weigh.astype(BF16)
     weigh_lo = (weigh - weigh_hi.astype(F32)).astype(BF16)
 
     whole(2, c_buf).wait_recv()
     rows = jnp.concatenate([p.astype(BF16) for p in gathered(c_buf)], axis=1)
-    flat = nt(w_all[4].reshape(32, 2048), jnp.concatenate([rows, rows], axis=0))
-    p_buf[chip] = jnp.where(lane < CHIPS, flat[0:16], flat[16:32]).astype(BF16)
+    swaps[4].wait_recv()
+    for copy in line_shares:
+        copy.wait_recv()
+    p_buf[chip] = nt(rows, w_mix[...].reshape(LANES, 2048)).astype(BF16)
     exchange(3, lambda there: p_buf.at[chip], p_buf)
 
     whole(3, p_buf).wait_recv()
-    halves = nt(both, p_buf[...].reshape(CHIPS * TILE, LANES))
-    projected = jnp.concatenate([halves[0:16], halves[16:32]], axis=1)
+    wide = jnp.concatenate([p_buf[4 * n : 4 * (n + 1)].reshape(CHIPS, LANES) for n in range(16)], axis=1)
+    projected = nn(select_line, wide)
     middle = (slot_tokens + projected).astype(BF16)
     middle32 = middle.astype(F32)
     scale = lax.rsqrt(jnp.mean(middle32 * middle32, axis=-1, keepdims=True) + EPS)
-    expert_in = (middle32 * scale * late_gain).astype(BF16).astype(F32)
+    expert_in = (middle32 * scale * expert_gain[...]).astype(BF16).astype(F32)
     e_rows[0] = expert_in[0:8]
     e_rows[1] = expert_in[8:16]
 
@@ -344,19 +377,15 @@
     rows_over = to_partner(5, e_rows.at[other], x_rows.at[core])
     rows_over.start()
     x_rows[core] = e_rows[core]
-    for load in gate_loads + up_loads + [down_load]:
+    for load in expert_loads:
         load.wait()
     rows_over.wait_recv()
     x = x_rows[...].reshape(16, 2048).astype(BF16)
     result = jnp.zeros((16, 2048), F32)
     for n in range(4):
         span = slice(256 * n, 256 * (n + 1))
-        gate_part = nn(x[:, :1024], gate_v[0, :, :, span].reshape(1024, 256)) + nn(
-            x[:, 1024:], gate_v[1, :, :, span].reshape(1024, 256)
-        )
-        up_part = nn(x[:, :1024], up_v[0, :, :, span].reshape(1024, 256)) + nn(
-            x[:, 1024:], up_v[1, :, :, span].reshape(1024, 256)
-        )
+        gate_part = nn(x, gate_v[:, span])
+        up_part = nn(x, up_v[:, span])
         hidden = (gate_part / (1.0 + jnp.exp(-gate_part)) * up_part).astype(BF16)
         result = result + nn(hidden, down_v[span, :])
     result = result.astype(BF16).astype(F32)
@@ -365,7 +394,7 @@
     rows_back = to_partner(6, r_send.at[other], r_rows.at[core])
     rows_back.start()
     r_rows[core] = r_send[core]
-    own_middle = restore(middle)[4:5]
+    own_middle = middle32[4:5]
     for s, piece in enumerate(pieces(own_middle)):
         tile32[s : s + 1, :] = piece
     rows_back.wait_recv()
@@ -385,10 +414,17 @@
 
     for phase, buf in enumerate((a_buf, b_buf, c_buf, p_buf, f_buf)):
         whole(phase, buf).wait_send()
-    for swap in swaps:
-        swap.wait_send()
-    rows_over.wait_send()
-    rows_back.wait_send()
+    for copy in swaps + line_sends + line_shares + [rows_over, rows_back]:
+        copy.wait_send()
+
+
+def finish(out_in, mem_in, norm_in, top_in, out, matrix, norm, top, sem):
+    stores = [pltpu.make_async_copy(mem_in.at[h], matrix.at[h], sem.at[h]) for h in range(4)]
+    for store in stores:
+        store.start()
+    out[...] = out_in[...]
+    norm[...] = norm_in[...]
+    top[...] = top_in[...]
     for store in stores:
         store.wait()
 
@@ -416,36 +452,41 @@
     group_weight,
     member_weight,
 ):
+    smem = pl.BlockSpec(memory_space=pltpu.SMEM)
     vmem = pl.BlockSpec(memory_space=pltpu.VMEM)
-    smem = pl.BlockSpec(memory_space=pltpu.SMEM)
-    hbm = pl.BlockSpec(memory_space=pl.ANY)
+    hbm = pl.BlockSpec(memory_space=pltpu.HBM)
     dma = pltpu.SemaphoreType.DMA
-    out, matrix, norm, top = pl.pallas_call(
+    sizes = ((1, 2048), BF16), ((4, 512, 512), F32), ((1, 4, 512), F32), ((1, 4), F32)
+    raw = pl.pallas_call(
         layer,
-        out_shape=(
-            jax.ShapeDtypeStruct((1, 2048), BF16),
-            jax.ShapeDtypeStruct((4, 512, 512), F32),
-            jax.ShapeDtypeStruct((1, 4, 512), F32),
-            jax.ShapeDtypeStruct((1, 4), F32),
-        ),
-        in_specs=[vmem, vmem, hbm, hbm, hbm, hbm, vmem, vmem, smem, hbm, vmem, smem, hbm, vmem, hbm, hbm, hbm, smem, smem, smem, smem],
-        out_specs=(vmem, hbm, vmem, vmem),
+        out_shape=tuple(pltpu.VMEM(*size) for size in sizes),
+        in_specs=[hbm] * 19 + [smem] * 2,
+        out_specs=(vmem,) * 4,
         scratch_shapes=[
-            pltpu.VMEM((5, 2, 16, 2048), BF16),
-            pltpu.VMEM((4, 512, 512), F32),
+            pltpu.VMEM((1, 2048), BF16),
+            pltpu.VMEM((1, 2048), F32),
+            pltpu.VMEM((4, 2048), BF16),
+            pltpu.VMEM((4, 2048), BF16),
+            pltpu.VMEM((1, 4, 512), F32),
+            pltpu.VMEM((1, 2048), F32),
+            pltpu.SMEM((4,), F32),
+            pltpu.SMEM((1, 4), F32),
+            pltpu.SMEM((1, 2), jnp.int32),
+            pltpu.SMEM((1, 2), F32),
+            pltpu.VMEM((4, 2, 16, 2048), BF16),
+            pltpu.VMEM((4, 2, 16, 2048), BF16),
             pltpu.VMEM((4, 512, 512), BF16),
-            pltpu.VMEM((2, CHIPS, 16, 1024), BF16),
-            pltpu.VMEM((2, CHIPS, 16, 1024), BF16),
+            pltpu.VMEM((2048, 1024), BF16),
+            pltpu.VMEM((2048, 1024), BF16),
             pltpu.VMEM((1024, 2048), BF16),
             pltpu.VMEM((LANES, 2048), BF16),
-            pltpu.VMEM((256, 256), BF16),
             pltpu.VMEM((CHIPS * TILE, LANES), F32),
             pltpu.VMEM((CHIPS, 2048), BF16),
             pltpu.VMEM((TILE, LANES), F32),
             pltpu.VMEM((CHIPS, TILE, LANES), BF16),
             pltpu.VMEM((CHIPS, 2, LANES), F32),
             pltpu.VMEM((CHIPS, 2, LANES), F32),
-            pltpu.VMEM((CHIPS, TILE, LANES), BF16),
+            pltpu.VMEM((CHIPS // 4, TILE, LANES), BF16),
             pltpu.VMEM((CHIPS, TILE, LANES), BF16),
             pltpu.VMEM((CHIPS, TILE, LANES), BF16),
             pltpu.VMEM((CHIPS, TILE, LANES), BF16),
@@ -455,13 +496,17 @@
             pltpu.VMEM((2, 8, 2048), F32),
             dma((5,)),
             dma((5,)),
-            dma((6,)),
+            dma((4,)),
+            dma((10,)),
             dma((5,)),
-            dma((4,)),
             dma((2, 7)),
+            dma((4, 3)),
         ],
-        compiler_params=pltpu.CompilerParams(collective_id=0, has_side_effects=True),
+        compiler_params=pltpu.CompilerParams(
+            collective_id=0, has_side_effects=True, vmem_limit_bytes=40 * 1024 * 1024
+        ),
     )(
+        *(pltpu.with_memory_space_constraint(value, pltpu.HBM) for value in (
         tokens,
         mixer_gain.reshape(1, 2048),
         query_weight.T,
@@ -476,14 +521,23 @@
         memory_max,
         mixer_out.T,
         expert_gain.reshape(1, 2048),
-        expert_gate.reshape(CHIPS, 2, 16, 1024),
-        expert_up.reshape(CHIPS, 2, 16, 1024),
+        expert_gate.reshape(2048, 1024),
+        expert_up.reshape(2048, 1024),
         expert_down.reshape(1024, 2048),
+        route_member,
+        member_weight,
+        )),
         route_group,
-        route_member,
         group_weight,
-        member_weight,
     )
+    out, matrix, norm, top = pl.pallas_call(
+        finish,
+        out_shape=tuple(jax.ShapeDtypeStruct(*size) for size in sizes),
+        in_specs=[vmem] * 4,
+        out_specs=(vmem, hbm, vmem, vmem),
+        scratch_shapes=[dma((4,))],
+        compiler_params=pltpu.CompilerParams(vmem_limit_bytes=8 * 1024 * 1024),
+    )(*(pltpu.with_memory_space_constraint(value, pltpu.VMEM) for value in raw))
     return out, matrix.reshape(1, 4, 512, 512), norm, top
 
 

time: 60 us -> 52.4 us (0.87)
  local copies, waits for them, and re-layouts: 7.07 us -> 0 us
    unnamed x8 -> x0, local copies, waits for them, and re-layouts: 7.07 us -> none
    pallas_call x1 -> x2, Pallas kernels: 50.8 us -> 50.3 us  [the longest x1 47.6 us: local(): pl.pallas_call(layer, out_shape=tuple((pltpu.VMEM(*size) for size in size...]
where the time goes in v2:
time: 52.4 us; the launch traced here: 52.2 us
  Pallas kernels  50.3 us (96%)
  between operations  1.94 us (4%)
    pallas_call x1, Pallas kernels, local(): pl.pallas_call(layer, out_shape=tuple((pltpu.VMEM(*size) for size in size...  47.6 us
    pallas_call x1, Pallas kernels, local(): pl.pallas_call(finish, out_shape=tuple((jax.ShapeDtypeStruct(*size) for s...  2.65 us

profile of v2, /device:TPU:0, one launch (start us, length us, event | category | flops | bytes accessed | tf_op | source)
XLA Modules:
  0.0 52.2 jit_solution(1052138979689195891)
XLA Ops:
  1.9 47.6 %shard_map.228 = (bf16[1,2048]{1,0:T(2,128)(2,1)S(1)}, f32[4,512,512]{2,1,0:T(8,128)S(1)}, f32[1,4,512]{2,1,0:T(4,128)S(1)}, f32[1,4]{1,0:T(1,128)S(1)}) custom-call(bf16[1,2048]{1,0:T(2,128)(2,1)} %tokens_in.1, f32[1,2048]{1,0:T(1,128)} %bitcast.25, bf16[16,2048]{1,0:T(8,128)(2,1)} %bitcast.18, bf16[16,2048]{1,0:T(8,128)(2,1)} %bitcast.19, ...), custom_call_target="tpu_custom_call" | custom-call | tf_op jit(solution)/shard_map/pallas_call | solution.py:460
  49.6 2.6 %shard_map.229 = (bf16[1,2048]{1,0:T(2,128)(2,1)}, f32[4,512,512]{2,1,0:T(8,128)}, f32[1,4,512]{2,1,0:T(4,128)}, f32[1,4]{1,0:T(1,128)}) custom-call(bf16[1,2048]{1,0:T(2,128)(2,1)S(1)} %get-tuple-element.12.out_in, f32[4,512,512]{2,1,0:T(8,128)S(1)} %get-tuple-element.13.mem_in, f32[1,4,512]{2,1,0:T(4,128)S(1)} %get-tuple-element.14.norm_in, ...), custom_call_target="tpu_custom_call" | custom-call | tf_op jit(solution)/shard_map/pallas_call | solution.py:533

commit v3 on v2

--- a/solution.py
+++ b/solution.py
@@ -109,18 +109,18 @@
     partner = me + 1 - 2 * core
     cz, cy, cx = lax.div(chip, 16), lax.rem(lax.div(chip, 4), 4), lax.rem(chip, 4)
 
-    def peer(i):
-        dz, dy, dx = lax.div(i, 16), lax.rem(lax.div(i, 4), 4), lax.rem(i, 4)
-        there = lax.rem(cz + dz, 4) * 16 + lax.rem(cy + dy, 4) * 4 + lax.rem(cx + dx, 4)
+    steps = [tuple(lax.rem(at + d, 4) * size for d in range(4)) for at, size in ((cz, 16), (cy, 4), (cx, 1))]
+    offsets = [(dz, dy, dx) for dz in range(4) for dy in range(4) for dx in range(4)][1:]
+    offsets.sort(key=lambda offset: -sum(min(d, 4 - d) for d in offset))
+
+    def peer(offset):
+        there = steps[0][offset[0]] + steps[1][offset[1]] + steps[2][offset[2]]
         return there, there * 2 + core
 
     barrier = pltpu.get_barrier_semaphore()
 
-    def greet(i, carry):
-        pl.semaphore_signal(barrier, inc=1, device_id=(peer(i)[1],), device_id_type=MESH)
-        return carry
-
-    lax.fori_loop(1, CHIPS, greet, 0)
+    for offset in offsets:
+        pl.semaphore_signal(barrier, inc=1, device_id=(peer(offset)[1],), device_id_type=MESH)
     pl.semaphore_signal(barrier, inc=1, device_id=(partner,), device_id_type=MESH)
 
     small = (
@@ -147,9 +147,11 @@
     for load in small_loads + own_loads + [mem_load] + expert_loads:
         load.start()
 
-    def exchange(phase, source, buf, stride=1, slot=chip):
-        def send(n, carry):
-            there, device = peer(CHIPS - stride * n)
+    def exchange(phase, source, buf, across=True, slot=chip):
+        for offset in offsets:
+            if offset[2] and not across:
+                continue
+            there, device = peer(offset)
             pltpu.make_async_remote_copy(
                 src_ref=source(there),
                 dst_ref=buf.at[slot],
@@ -158,9 +160,6 @@
                 device_id=(device,),
                 device_id_type=MESH,
             ).start()
-            return carry
-
-        lax.fori_loop(1, CHIPS // stride, send, 0)
 
     def whole(phase, buf):
         span = buf.at[pl.ds(0, buf.shape[0] - 1)]
@@ -295,7 +294,7 @@
         tile32[pl.ds(b, 4, stride=4), :] = gated[:, LANES * b : LANES * (b + 1)]
     spot = lax.div(chip, 4)
     c_buf[spot] = tile32[...].astype(BF16)
-    exchange(2, lambda there: c_buf.at[spot], c_buf, 4, spot)
+    exchange(2, lambda there: c_buf.at[spot], c_buf, False, spot)
 
     line_shares = []
     for n, copy in enumerate(line_sends):
@@ -381,13 +380,10 @@
         load.wait()
     rows_over.wait_recv()
     x = x_rows[...].reshape(16, 2048).astype(BF16)
-    result = jnp.zeros((16, 2048), F32)
-    for n in range(4):
-        span = slice(256 * n, 256 * (n + 1))
-        gate_part = nn(x, gate_v[:, span])
-        up_part = nn(x, up_v[:, span])
-        hidden = (gate_part / (1.0 + jnp.exp(-gate_part)) * up_part).astype(BF16)
-        result = result + nn(hidden, down_v[span, :])
+    gate_part = nn(x, gate_v[...])
+    up_part = nn(x, up_v[...])
+    hidden = (gate_part / (1.0 + jnp.exp(-gate_part)) * up_part).astype(BF16)
+    result = nn(hidden, down_v[...])
     result = result.astype(BF16).astype(F32)
     r_send[0] = result[0:8]
     r_send[1] = result[8:16]
@@ -419,14 +415,17 @@
 
 
 def finish(out_in, mem_in, norm_in, top_in, out, matrix, norm, top, sem):
-    stores = [pltpu.make_async_copy(mem_in.at[h], matrix.at[h], sem.at[h]) for h in range(4)]
-    for store in stores:
-        store.start()
-    out[...] = out_in[...]
-    norm[...] = norm_in[...]
-    top[...] = top_in[...]
-    for store in stores:
-        store.wait()
+    copies = [
+        pltpu.make_async_copy(mem_in.at[h, pl.ds(256 * n, 256)], matrix.at[h, pl.ds(256 * n, 256)], sem.at[2 * h + n])
+        for h in range(4)
+        for n in range(2)
+    ]
+    for n, (source, target) in enumerate(((out_in, out), (norm_in, norm), (top_in, top))):
+        copies.append(pltpu.make_async_copy(source, target, sem.at[8 + n]))
+    for copy in copies:
+        copy.start()
+    for copy in copies:
+        copy.wait()
 
 
 def local(
@@ -534,8 +533,8 @@
         finish,
         out_shape=tuple(jax.ShapeDtypeStruct(*size) for size in sizes),
         in_specs=[vmem] * 4,
-        out_specs=(vmem, hbm, vmem, vmem),
-        scratch_shapes=[dma((4,))],
+        out_specs=(hbm,) * 4,
+        scratch_shapes=[dma((11,))],
         compiler_params=pltpu.CompilerParams(vmem_limit_bytes=8 * 1024 * 1024),
     )(*(pltpu.with_memory_space_constraint(value, pltpu.VMEM) for value in raw))
     return out, matrix.reshape(1, 4, 512, 512), norm, top

time: 52.4 us -> 49.2 us (0.939)
  Pallas kernels: 50.3 us -> 47.1 us
    pallas_call x1, Pallas kernels: 47.6 us -> 45 us  [local(): pl.pallas_call(layer, out_shape=tuple((pltpu.VMEM(*size) for size in size...]
    pallas_call x1, Pallas kernels: 2.65 us -> 2.11 us  [local(): pl.pallas_call(finish, out_shape=tuple((jax.ShapeDtypeStruct(*size) for s...]
where the time goes in v3:
time: 49.2 us; the launch traced here: 49.1 us
  Pallas kernels  47.1 us (96%)
  between operations  1.94 us (4%)
    pallas_call x1, Pallas kernels, local(): pl.pallas_call(layer, out_shape=tuple((pltpu.VMEM(*size) for size in size...  45 us
    pallas_call x1, Pallas kernels, local(): pl.pallas_call(finish, out_shape=tuple((jax.ShapeDtypeStruct(*size) for s...  2.11 us

profile of v3, /device:TPU:0, one launch (start us, length us, event | category | flops | bytes accessed | tf_op | source)
XLA Modules:
  0.0 49.1 jit_solution(6722594430772558205)
XLA Ops:
  1.9 45.0 %shard_map.228 = (bf16[1,2048]{1,0:T(2,128)(2,1)S(1)}, f32[4,512,512]{2,1,0:T(8,128)S(1)}, f32[1,4,512]{2,1,0:T(4,128)S(1)}, f32[1,4]{1,0:T(1,128)S(1)}) custom-call(bf16[1,2048]{1,0:T(2,128)(2,1)} %tokens_in.1, f32[1,2048]{1,0:T(1,128)} %bitcast.25, bf16[16,2048]{1,0:T(8,128)(2,1)} %bitcast.18, bf16[16,2048]{1,0:T(8,128)(2,1)} %bitcast.19, ...), custom_call_target="tpu_custom_call" | custom-call | tf_op jit(solution)/shard_map/pallas_call | solution.py:459
  47.0 2.1 %shard_map.229 = (bf16[1,2048]{1,0:T(2,128)(2,1)}, f32[4,512,512]{2,1,0:T(8,128)}, f32[1,4,512]{2,1,0:T(4,128)}, f32[1,4]{1,0:T(1,128)}) custom-call(bf16[1,2048]{1,0:T(2,128)(2,1)S(1)} %get-tuple-element.12.out_in, f32[4,512,512]{2,1,0:T(8,128)S(1)} %get-tuple-element.13.mem_in, f32[1,4,512]{2,1,0:T(4,128)S(1)} %get-tuple-element.14.norm_in, ...), custom_call_target="tpu_custom_call" | custom-call | tf_op jit(solution)/shard_map/pallas_call | solution.py:532

commit v4 on v3

--- a/solution.py
+++ b/solution.py
@@ -112,6 +112,7 @@
     steps = [tuple(lax.rem(at + d, 4) * size for d in range(4)) for at, size in ((cz, 16), (cy, 4), (cx, 1))]
     offsets = [(dz, dy, dx) for dz in range(4) for dy in range(4) for dx in range(4)][1:]
     offsets.sort(key=lambda offset: -sum(min(d, 4 - d) for d in offset))
+    offsets.sort(key=lambda offset: -sum(min(d, 4 - d) for d in offset[:2]))
 
     def peer(offset):
         there = steps[0][offset[0]] + steps[1][offset[1]] + steps[2][offset[2]]
@@ -342,8 +343,8 @@
     by_line = (b == lax.rem(a, 4) * 16 + lax.div(a, 4)).astype(F32).astype(BF16)
     select_line = nn(select, by_line).astype(BF16)
     weigh = weigh[:, :16]
-    weigh_hi = weigh.astype(BF16)
-    weigh_lo = (weigh - weigh_hi.astype(F32)).astype(BF16)
+    weigh_hi = weigh.astype(BF16).astype(F32)
+    weights = jnp.concatenate([weigh_hi, weigh - weigh_hi], axis=1).astype(BF16)
 
     whole(2, c_buf).wait_recv()
     rows = jnp.concatenate([p.astype(BF16) for p in gathered(c_buf)], axis=1)
@@ -396,22 +397,24 @@
     rows_back.wait_recv()
 
     slots = r_rows[...].reshape(16, 2048).astype(BF16)
-    mixed = nn(weigh_hi, slots) + nn(weigh_lo, slots)
-    for s, piece in enumerate(pieces(mixed)):
-        rows32[pl.ds(s, CHIPS, stride=TILE), :] = piece
+    slots = jnp.concatenate([slots, slots], axis=0)
+    for n in range(8):
+        mixed = nn(weights, slots[:, 256 * n : 256 * (n + 1)])
+        for s, piece in enumerate(pieces(mixed)):
+            rows32[pl.ds(2 * n + s, CHIPS, stride=TILE), :] = piece
     f_src[...] = rows32[...].reshape(CHIPS, TILE, LANES).astype(BF16)
     exchange(4, lambda there: f_src.at[there], f_buf)
     f_buf[chip] = f_src[chip]
+    for phase, buf in enumerate((a_buf, b_buf, c_buf, p_buf)):
+        whole(phase, buf).wait_send()
+    for copy in swaps + line_sends + line_shares + [rows_over, rows_back]:
+        copy.wait_send()
     whole(4, f_buf).wait_recv()
     total = tile32[...] + jnp.sum(f_buf[...].astype(F32), axis=0)
     final = total.astype(BF16).astype(F32)
     for s in range(TILE):
         out_ref[:, LANES * s : LANES * (s + 1)] = final[s : s + 1].astype(BF16)
-
-    for phase, buf in enumerate((a_buf, b_buf, c_buf, p_buf, f_buf)):
-        whole(phase, buf).wait_send()
-    for copy in swaps + line_sends + line_shares + [rows_over, rows_back]:
-        copy.wait_send()
+    whole(4, f_buf).wait_send()
 
 
 def finish(out_in, mem_in, norm_in, top_in, out, matrix, norm, top, sem):

time: 49.2 us -> 48.8 us (level)
  no operation moved by 1% of the time
where the time goes in v4:
time: 48.8 us; the launch traced here: 48.7 us
  Pallas kernels  46.7 us (96%)
  between operations  1.94 us (4%)
    pallas_call x1, Pallas kernels, local(): pl.pallas_call(layer, out_shape=tuple((pltpu.VMEM(*size) for size in size...  44.6 us
    pallas_call x1, Pallas kernels, local(): pl.pallas_call(finish, out_shape=tuple((jax.ShapeDtypeStruct(*size) for s...  2.11 us

profile of v4, /device:TPU:0, one launch (start us, length us, event | category | flops | bytes accessed | tf_op | source)
XLA Modules:
  0.0 48.7 jit_solution(16821430790702868168)
XLA Ops:
  1.9 44.6 %shard_map.228 = (bf16[1,2048]{1,0:T(2,128)(2,1)S(1)}, f32[4,512,512]{2,1,0:T(8,128)S(1)}, f32[1,4,512]{2,1,0:T(4,128)S(1)}, f32[1,4]{1,0:T(1,128)S(1)}) custom-call(bf16[1,2048]{1,0:T(2,128)(2,1)} %tokens_in.1, f32[1,2048]{1,0:T(1,128)} %bitcast.25, bf16[16,2048]{1,0:T(8,128)(2,1)} %bitcast.18, bf16[16,2048]{1,0:T(8,128)(2,1)} %bitcast.19, ...), custom_call_target="tpu_custom_call" | custom-call | tf_op jit(solution)/shard_map/pallas_call | solution.py:462
  46.5 2.1 %shard_map.229 = (bf16[1,2048]{1,0:T(2,128)(2,1)}, f32[4,512,512]{2,1,0:T(8,128)}, f32[1,4,512]{2,1,0:T(4,128)}, f32[1,4]{1,0:T(1,128)}) custom-call(bf16[1,2048]{1,0:T(2,128)(2,1)S(1)} %get-tuple-element.12.out_in, f32[4,512,512]{2,1,0:T(8,128)S(1)} %get-tuple-element.13.mem_in, f32[1,4,512]{2,1,0:T(4,128)S(1)} %get-tuple-element.14.norm_in, ...), custom_call_target="tpu_custom_call" | custom-call | tf_op jit(solution)/shard_map/pallas_call | solution.py:535
